TPU v7x, 32 devices: a whole 2x2x4 slice. The times are simulated.
32 devices in a mesh: fs: 8 (over z, y), tp: 4 (over x, core).
Axes of the slice: x: 2, y: 2, z: 4, core: 2. Of those that a mesh axis runs over, the one named last changes fastest.
Arguments:
- prompt_tokens: bfloat16 [768, 4096], P('tp'), may hold values from -6 to 6
- norm_gain: float32 [4096], P('fs'), may hold values from 0.1 to 1.9
- gate_trained: float32 [4096, 11264], P('fs', 'tp'), may hold values from -0.09375 to 0.09375
- up_trained: float32 [4096, 11264], P('fs', 'tp'), may hold values from -0.09375 to 0.09375
- down_trained: float32 [11264, 4096], P('fs', 'tp'), may hold values from -0.078125 to 0.078125
Outputs:
- gate_serving: bfloat16 [4096, 11264], P(None, 'fs')
- up_serving: bfloat16 [4096, 11264], P(None, 'fs')
- down_serving: bfloat16 [11264, 4096], P('fs')
- mixed: bfloat16 [768, 4096], P('tp', 'fs')
All inputs are finite; a program needn't handle non-finite values.
Results may differ from a plain program's by a relative error of at most 0.0082.
Values may be sent and summed in bfloat16 or wider, within the bound.
A program may use at most 128 MiB of HBM per device.

v0:
```python
import jax
import jax.numpy as jnp
from jax import lax
from jax.sharding import PartitionSpec as P


def on_device(prompt_tokens, norm_gain, gate_trained, up_trained, down_trained):
    fs_count = lax.axis_size("fs")
    gate_cast = (gate_trained * norm_gain[:, None]).astype(jnp.bfloat16)
    up_cast = (up_trained * norm_gain[:, None]).astype(jnp.bfloat16)
    down_cast = down_trained.astype(jnp.bfloat16)
    down_serving = lax.all_gather(down_cast, "tp", axis=1, tiled=True)
    gate_part, up_part = (
        lax.all_to_all(gate_cast, "tp", split_axis=0, concat_axis=1, tiled=True),
        lax.all_to_all(up_cast, "tp", split_axis=0, concat_axis=1, tiled=True),
    )
    gate_mid, up_mid = (
        lax.all_to_all(gate_part, "fs", split_axis=1, concat_axis=0, tiled=True),
        lax.all_to_all(up_part, "fs", split_axis=1, concat_axis=0, tiled=True),
    )
    share = gate_mid.shape[0] // fs_count
    width = gate_mid.shape[1]
    gate_blocks, up_blocks = (
        lax.all_gather(gate_mid.reshape(fs_count, share, width), "tp", axis=1, tiled=True),
        lax.all_gather(up_mid.reshape(fs_count, share, width), "tp", axis=1, tiled=True),
    )
    gate_serving = gate_blocks.reshape(-1, width)
    up_serving = up_blocks.reshape(-1, width)
    tokens = prompt_tokens.astype(jnp.float32)
    scale = lax.rsqrt(jnp.mean(tokens * tokens, axis=-1, keepdims=True) + 1e-06)
    normed = (tokens * scale).astype(jnp.bfloat16)
    contract = (((0,), (1,)), ((), ()))
    gate_cols = lax.dot_general(gate_serving, normed, contract, preferred_element_type=jnp.float32)
    up_cols = lax.dot_general(up_serving, normed, contract, preferred_element_type=jnp.float32)
    hidden_cols = (jax.nn.silu(gate_cols) * up_cols).astype(jnp.bfloat16)
    summed = lax.psum_scatter(
        lax.dot_general(
            down_serving, hidden_cols, (((0,), (0,)), ((), ())), preferred_element_type=jnp.float32
        ),
        "fs",
        scatter_dimension=0,
        tiled=True,
    )
    mixed = summed.T.astype(jnp.bfloat16)
    return (gate_serving, up_serving, down_serving, mixed)


def solution(mesh):
    return jax.shard_map(
        on_device,
        mesh=mesh,
        in_specs=(P("tp", None), P("fs"), P("fs", "tp"), P("fs", "tp"), P("fs", "tp")),
        out_specs=(P(None, "fs"), P(None, "fs"), P("fs", None), P("tp", "fs")),
        check_vma=False,
    )
```

profile of v0, /device:TPU:0, one launch (start us, length us, event | category | flops | bytes accessed | tf_op | source)
XLA Modules:
  0.0 524.6 jit_solution(6554279546055345411)
XLA Ops:
  7.2 0.0 all-gather.4.cloned.1.call-start
  7.2 5.5 %multiply_convert_fusion = (bf16[512,2816]{1,0:T(8,128)(2,1)S(1)}, bf16[512,2816]{1,0:T(8,128)(2,1)S(1)}) fusion(f32[512,2816]{1,0:T(8,128)} %param.8, f32[512]{0:T(512)} %param.6, f32[512,2816]{1,0:T(8,128)} %param.7), kind=kLoop, calls=%fused_computation | loop fusion | flops 5767168 | bytes 17303552 | tf_op jit(solution)/shard_map/convert_element_type | solution.py:10
  12.7 38.2 %all_to_all.64 = bf16[4,128,2816]{2,1,0:T(8,128)(2,1)} all-to-all(bf16[4,128,2816]{2,1,0:T(8,128)(2,1)S(1)} %bitcast.18), channel_id=1, replica_groups=mesh['fs'=8,'tp'=4] {'tp'}, dimensions={0} | all-to-all | bytes 5767168 | tf_op jit(solution)/shard_map/all_to_all | solution.py:14
  51.0 4.5 copy.9
  55.5 71.4 %all_to_all.65 = bf16[128,8,1408]{0,2,1:T(8,128)(2,1)} all-to-all(bf16[128,8,1408]{0,2,1:T(8,128)(2,1)} %bitcast.26), channel_id=1, replica_groups=mesh['fs'=8,'tp'=4] {'fs'}, dimensions={1} | all-to-all | bytes 5767168 | tf_op jit(solution)/shard_map/all_to_all | solution.py:18
  126.9 0.0 all-gather.4.cloned.1.call-update
  126.9 0.0 all-gather.6.cloned.1.call-start
  127.0 64.5 %all_to_all.66 = bf16[4,128,2816]{2,1,0:T(8,128)(2,1)} all-to-all(bf16[4,128,2816]{2,1,0:T(8,128)(2,1)S(1)} %bitcast.17), channel_id=1, replica_groups=mesh['fs'=8,'tp'=4] {'tp'}, dimensions={0} | all-to-all | bytes 5767168 | tf_op jit(solution)/shard_map/all_to_all | solution.py:15
  191.5 3.3 copy.11
  194.8 67.9 %all_to_all.67 = bf16[128,8,1408]{0,2,1:T(8,128)(2,1)} all-to-all(bf16[128,8,1408]{0,2,1:T(8,128)(2,1)S(1)} %bitcast.28), channel_id=1, replica_groups=mesh['fs'=8,'tp'=4] {'fs'}, dimensions={1} | all-to-all | bytes 5767168 | tf_op jit(solution)/shard_map/all_to_all | solution.py:19
  262.8 0.0 all-gather.8.cloned.1.call-start
  262.8 4.7 convert_element_type.26
  267.5 0.0 reduce-scatter.2.cloned.1.call-start
  267.6 1.6 copy-done
  269.1 0.4 fusion
  269.6 16.0 %copy.10 = bf16[8,512,1408]{2,1,0:T(8,128)(2,1)} copy(bf16[8,512,1408]{1,2,0:T(8,128)(2,1)} %all-gather.4.cloned.1.call-done) | data formatting | bytes 23068672 | tf_op jit(solution)/shard_map/all_gather | solution.py:24
  285.6 53.0 %all-gather.6.cloned.1.call-done = bf16[8,512,1408]{1,2,0:T(8,128)(2,1)} async-done(((bf16[8,128,1408]{1,2,0:T(8,128)(2,1)}), bf16[8,512,1408]{1,2,0:T(8,128)(2,1)}) %all-gather.6.cloned.1.call-update) | async-done | bytes 11534352 | tf_op jit(solution)/shard_map/all_gather | solution.py:25
  338.5 16.0 %copy.12 = bf16[8,512,1408]{2,1,0:T(8,128)(2,1)} copy(bf16[8,512,1408]{1,2,0:T(8,128)(2,1)} %all-gather.6.cloned.1.call-done) | data formatting | bytes 23068672 | tf_op jit(solution)/shard_map/all_gather | solution.py:25
  354.5 7.2 %fusion.3 = f32[1408,192]{0,1:T(8,128)S(1)} fusion(bf16[4096,1408]{1,0:T(8,128)(2,1)} %bitcast.19, bf16[192,4096]{1,0:T(8,128)(2,1)S(1)} %copy-done, f32[192]{0:T(256)S(1)} %add_rsqrt_fusion), kind=kOutput, calls=%fused_computation.9 | convolution fusion | flops 2216951808 | bytes 14189312 | tf_op jit(solution)/shard_map/dot_general | solution.py:33
  361.8 55.1 %all-gather.8.cloned.1.call-done = bf16[1408,4096]{1,0:T(8,128)(2,1)} async-done(((bf16[1408,1024]{1,0:T(8,128)(2,1)}), bf16[1408,4096]{1,0:T(8,128)(2,1)}) %all-gather.8.cloned.1.call-update) | async-done | bytes 11534352 | tf_op jit(solution)/shard_map/all_gather | solution.py:12
  416.8 14.4 %convolution_bitcast_fusion = f32[4096,192]{0,1:T(8,128)} fusion(bf16[1408,4096]{1,0:T(8,128)(2,1)} %all-gather.8.cloned.1.call-done, bf16[4096,1408]{1,0:T(8,128)(2,1)} %bitcast.21, f32[1408,192]{0,1:T(8,128)S(1)} %fusion.3, bf16[192,4096]{1,0:T(8,128)(2,1)S(1)} %copy-done, f32[192]{0:T(256)S(1)} %add_rsqrt_fusion), kind=kOutput, calls=%fused_computation.2 | convolution fusion | flops 4433166336 | bytes 28869376 | tf_op jit(solution)/shard_map/dot_general | solution.py:37
  431.3 75.0 %reduce-scatter.2.cloned.1.call-done = f32[512,192]{0,1:T(8,128)} async-done(((f32[4096,192]{0,1:T(8,128)}), f32[512,192]{0,1:T(8,128)}) %reduce-scatter.2.cloned.1.call-update) | async-done | bytes 393232 | tf_op jit(solution)/shard_map/reduce_scatter | solution.py:36
  506.3 1.7 convert_bitcast_fusion
  508.0 10.1 %copy.14 = bf16[1408,4096]{1,0:T(8,128)(2,1)} copy(bf16[1408,4096]{1,0:T(8,128)(2,1)} %all-gather.8.cloned.1.call-done) | data formatting | bytes 23068672
  (6 shorter events, 0.1 us)
Async XLA Ops:
  7.2 262.4 %all-gather.4.cloned.1.call-start = ((), (), s32[]{:S(2)}) async-start(), calls=%async_computation.5 | async-start | bytes 14417920 | tf_op jit(solution)/shard_map/all_gather | solution.py:24
  126.9 211.6 %all-gather.6.cloned.1.call-start = ((), (), s32[]{:S(2)}) async-start(), calls=%async_computation.6 | async-start | bytes 14417920 | tf_op jit(solution)/shard_map/all_gather | solution.py:25
  262.8 154.1 %all-gather.8.cloned.1.call-start = ((), (), s32[]{:S(2)}) async-start(), calls=%async_computation.7 | async-start | bytes 14417920 | tf_op jit(solution)/shard_map/all_gather | solution.py:12
  267.5 1.6 copy-start
  267.5 238.8 %reduce-scatter.2.cloned.1.call-start = ((), (), s32[]{:S(2)}) async-start(), calls=%async_computation.8 | async-start | bytes 3538944 | tf_op jit(solution)/shard_map/reduce_scatter | solution.py:36
Sparse Core Ops, SparseCore 0:
  127.1 102.4 all-gather.3
  262.9 75.5 all-gather.5
  340.7 76.1 all-gather.7
  431.4 74.8 reduce-scatter.1
where the time goes:
time: 526 us; the launch traced here: 525 us
  blocking collectives  242 us (46%)
  waiting for transfers between devices  183 us (35%)
  local copies, waits for them, and re-layouts  51.5 us (10%)
  matrix products  21.7 us (4%)
  between operations  13.8 us (3%)
  other arithmetic  12.3 us (2%)
    reduce_scatter x1, waiting for transfers between devices, on_device(): lax.psum_scatter(lax.dot_general(down_serving, hidden_cols, (((0,), (0,))...  75 us
    all_to_all x1, blocking collectives, on_device(): lax.all_to_all(gate_part, 'fs', split_axis=1, concat_axis=0, tiled=True)  71.4 us
    all_to_all x1, blocking collectives, on_device(): lax.all_to_all(up_part, 'fs', split_axis=1, concat_axis=0, tiled=True)  67.9 us
    all_to_all x1, blocking collectives, on_device(): lax.all_to_all(up_cast, 'tp', split_axis=0, concat_axis=1, tiled=True)  64.5 us
    all_gather x1, waiting for transfers between devices, on_device(): down_serving = lax.all_gather(down_cast, 'tp', axis=1, tiled=True)  55.1 us
    all_gather x1, waiting for transfers between devices, on_device(): lax.all_gather(up_mid.reshape(fs_count, share, width), 'tp', axis=1, tile...  53 us
    all_to_all x1, blocking collectives, on_device(): lax.all_to_all(gate_cast, 'tp', split_axis=0, concat_axis=1, tiled=True)  38.2 us
    all_gather x1, local copies, waits for them, and re-layouts, on_device(): lax.all_gather(up_mid.reshape(fs_count, share, width), 'tp', axis=1, tile...  16 us
  transfers between devices with their start and end apart: 4, of which 3 were waited for; matrix products, arithmetic and copies ran while one was open for 9% of the time, Pallas kernels for 0%

commit v1 on v0

--- a/solution.py
+++ b/solution.py
@@ -12,7 +12,10 @@
     down_serving = lax.all_gather(down_cast, "tp", axis=1, tiled=True)
     gate_part, up_part = (
         lax.all_to_all(gate_cast, "tp", split_axis=0, concat_axis=1, tiled=True),
-        lax.all_to_all(up_cast, "tp", split_axis=0, concat_axis=1, tiled=True),
+        jnp.concatenate(
+            lax.all_to_all(jnp.stack(jnp.split(up_cast, lax.axis_size("tp"), axis=0)), "tp", 0, 0),
+            axis=1,
+        ),
     )
     gate_mid, up_mid = (
         lax.all_to_all(gate_part, "fs", split_axis=1, concat_axis=0, tiled=True),

time: 526 us -> 527 us (level)
    all_gather x1, waiting for transfers between devices: 0.02 us -> 53 us  [on_device(): lax.all_gather(gate_mid.reshape(fs_count, share, width), 'tp', axis=1, ti...]
    all_gather x1, waiting for transfers between devices: 53 us -> 0.02 us  [on_device(): lax.all_gather(up_mid.reshape(fs_count, share, width), 'tp', axis=1, tile...]
    all_to_all x1, blocking collectives: 64.5 us -> 38.2 us  [on_device(): lax.all_to_all(jnp.stack(jnp.split(up_cast, lax.axis_size('tp'), axis=0))...]
    all_to_all x1, blocking collectives: 38.2 us -> 64.5 us  [on_device(): lax.all_to_all(gate_cast, 'tp', split_axis=0, concat_axis=1, tiled=True)]
where the time goes in v1:
time: 527 us; the launch traced here: 525 us
  blocking collectives  242 us (46%)
  waiting for transfers between devices  183 us (35%)
  local copies, waits for them, and re-layouts  51.7 us (10%)
  matrix products  21.7 us (4%)
  between operations  13.8 us (3%)
  other arithmetic  12.7 us (2%)
    reduce_scatter x1, waiting for transfers between devices, on_device(): lax.psum_scatter(lax.dot_general(down_serving, hidden_cols, (((0,), (0,))...  74.9 us
    all_to_all x1, blocking collectives, on_device(): lax.all_to_all(up_part, 'fs', split_axis=1, concat_axis=0, tiled=True)  71.4 us
    all_to_all x1, blocking collectives, on_device(): lax.all_to_all(gate_part, 'fs', split_axis=1, concat_axis=0, tiled=True)  67.9 us
    all_to_all x1, blocking collectives, on_device(): lax.all_to_all(gate_cast, 'tp', split_axis=0, concat_axis=1, tiled=True)  64.5 us
    all_gather x1, waiting for transfers between devices, on_device(): down_serving = lax.all_gather(down_cast, 'tp', axis=1, tiled=True)  55.1 us
    all_gather x1, waiting for transfers between devices, on_device(): lax.all_gather(gate_mid.reshape(fs_count, share, width), 'tp', axis=1, ti...  53 us
    all_to_all x1, blocking collectives, on_device(): lax.all_to_all(jnp.stack(jnp.split(up_cast, lax.axis_size('tp'), axis=0))...  38.2 us
    all_gather x1, local copies, waits for them, and re-layouts, on_device(): lax.all_gather(gate_mid.reshape(fs_count, share, width), 'tp', axis=1, ti...  16 us
  transfers between devices with their start and end apart: 4, of which 3 were waited for; matrix products, arithmetic and copies ran while one was open for 9% of the time, Pallas kernels for 0%

profile of v1, /device:TPU:0, one launch (start us, length us, event | category | flops | bytes accessed | tf_op | source)
XLA Modules:
  0.0 525.1 jit_solution(10907129693258896860)
XLA Ops:
  7.2 5.5 %multiply_convert_fusion = (bf16[512,2816]{1,0:T(8,128)(2,1)S(1)}, bf16[512,2816]{1,0:T(8,128)(2,1)S(1)}) fusion(f32[512,2816]{1,0:T(8,128)} %param.8, f32[512]{0:T(512)} %param.6, f32[512,2816]{1,0:T(8,128)} %param.7), kind=kLoop, calls=%fused_computation | loop fusion | flops 5767168 | bytes 17303552 | tf_op jit(solution)/shard_map/convert_element_type | solution.py:10
  12.7 0.2 slice_bitcast_fusion.3
  12.9 0.4 pad_maximum_fusion
  13.3 38.2 %all_to_all.53 = bf16[4,128,2816]{2,1,0:T(8,128)(2,1)} all-to-all(bf16[4,128,2816]{2,1,0:T(8,128)(2,1)S(1)} %pad_maximum_fusion), channel_id=1, replica_groups=mesh['fs'=8,'tp'=4] {'tp'}, dimensions={0} | all-to-all | bytes 5767168 | tf_op jit(solution)/shard_map/all_to_all | solution.py:16
  51.6 4.5 copy.13
  56.1 71.4 %all_to_all.54 = bf16[128,8,1408]{0,2,1:T(8,128)(2,1)} all-to-all(bf16[128,8,1408]{0,2,1:T(8,128)(2,1)} %bitcast.32), channel_id=1, replica_groups=mesh['fs'=8,'tp'=4] {'fs'}, dimensions={1} | all-to-all | bytes 5767168 | tf_op jit(solution)/shard_map/all_to_all | solution.py:22
  127.6 0.0 all-gather.4.cloned.1.call-start
  127.6 64.5 %all_to_all.55 = bf16[4,128,2816]{2,1,0:T(8,128)(2,1)} all-to-all(bf16[4,128,2816]{2,1,0:T(8,128)(2,1)S(1)} %bitcast.24), channel_id=1, replica_groups=mesh['fs'=8,'tp'=4] {'tp'}, dimensions={0} | all-to-all | bytes 5767168 | tf_op jit(solution)/shard_map/all_to_all | solution.py:14
  192.1 3.3 copy.11
  195.4 67.9 %all_to_all.56 = bf16[128,8,1408]{0,2,1:T(8,128)(2,1)} all-to-all(bf16[128,8,1408]{0,2,1:T(8,128)(2,1)S(1)} %bitcast.34), channel_id=1, replica_groups=mesh['fs'=8,'tp'=4] {'fs'}, dimensions={1} | all-to-all | bytes 5767168 | tf_op jit(solution)/shard_map/all_to_all | solution.py:21
  263.4 0.0 all-gather.8.cloned.1.call-start
  263.4 4.7 convert_element_type.26
  268.1 0.0 reduce-scatter.2.cloned.1.call-start
  268.2 1.6 copy-done
  269.8 0.4 fusion
  270.2 16.0 %copy.14 = bf16[8,512,1408]{2,1,0:T(8,128)(2,1)} copy(bf16[8,512,1408]{1,2,0:T(8,128)(2,1)} %all-gather.6.cloned.1.call-done) | data formatting | bytes 23068672 | tf_op jit(solution)/shard_map/all_gather | solution.py:28
  286.2 53.0 %all-gather.4.cloned.1.call-done = bf16[8,512,1408]{1,2,0:T(8,128)(2,1)} async-done(((bf16[8,128,1408]{1,2,0:T(8,128)(2,1)}), bf16[8,512,1408]{1,2,0:T(8,128)(2,1)}) %all-gather.4.cloned.1.call-update) | async-done | bytes 11534352 | tf_op jit(solution)/shard_map/all_gather | solution.py:27
  339.2 16.0 %copy.12 = bf16[8,512,1408]{2,1,0:T(8,128)(2,1)} copy(bf16[8,512,1408]{1,2,0:T(8,128)(2,1)} %all-gather.4.cloned.1.call-done) | data formatting | bytes 23068672 | tf_op jit(solution)/shard_map/all_gather | solution.py:27
  355.2 7.2 %fusion.3 = f32[1408,192]{0,1:T(8,128)S(1)} fusion(bf16[4096,1408]{1,0:T(8,128)(2,1)} %bitcast.27, bf16[192,4096]{1,0:T(8,128)(2,1)S(1)} %copy-done, f32[192]{0:T(256)S(1)} %add_rsqrt_fusion), kind=kOutput, calls=%fused_computation.14 | convolution fusion | flops 2216951808 | bytes 14189312 | tf_op jit(solution)/shard_map/dot_general | solution.py:36
  362.4 55.1 %all-gather.8.cloned.1.call-done = bf16[1408,4096]{1,0:T(8,128)(2,1)} async-done(((bf16[1408,1024]{1,0:T(8,128)(2,1)}), bf16[1408,4096]{1,0:T(8,128)(2,1)}) %all-gather.8.cloned.1.call-update) | async-done | bytes 11534352 | tf_op jit(solution)/shard_map/all_gather | solution.py:12
  417.5 14.4 %convolution_bitcast_fusion = f32[4096,192]{0,1:T(8,128)} fusion(bf16[1408,4096]{1,0:T(8,128)(2,1)} %all-gather.8.cloned.1.call-done, bf16[4096,1408]{1,0:T(8,128)(2,1)} %bitcast.25, f32[1408,192]{0,1:T(8,128)S(1)} %fusion.3, bf16[192,4096]{1,0:T(8,128)(2,1)S(1)} %copy-done, f32[192]{0:T(256)S(1)} %add_rsqrt_fusion), kind=kOutput, calls=%fused_computation.2 | convolution fusion | flops 4433166336 | bytes 28869376 | tf_op jit(solution)/shard_map/dot_general | solution.py:40
  431.9 74.9 %reduce-scatter.2.cloned.1.call-done = f32[512,192]{0,1:T(8,128)} async-done(((f32[4096,192]{0,1:T(8,128)}), f32[512,192]{0,1:T(8,128)}) %reduce-scatter.2.cloned.1.call-update) | async-done | bytes 393232 | tf_op jit(solution)/shard_map/reduce_scatter | solution.py:39
  506.8 1.7 convert_bitcast_fusion
  508.5 10.1 %copy.16 = bf16[1408,4096]{1,0:T(8,128)(2,1)} copy(bf16[1408,4096]{1,0:T(8,128)(2,1)} %all-gather.8.cloned.1.call-done) | data formatting | bytes 23068672
  (8 shorter events, 0.1 us)
Async XLA Ops:
  7.2 263.0 %all-gather.6.cloned.1.call-start = ((), (), s32[]{:S(2)}) async-start(), calls=%async_computation.6 | async-start | bytes 14417920 | tf_op jit(solution)/shard_map/all_gather | solution.py:28
  127.6 211.6 %all-gather.4.cloned.1.call-start = ((), (), s32[]{:S(2)}) async-start(), calls=%async_computation.5 | async-start | bytes 14417920 | tf_op jit(solution)/shard_map/all_gather | solution.py:27
  263.4 154.1 %all-gather.8.cloned.1.call-start = ((), (), s32[]{:S(2)}) async-start(), calls=%async_computation.7 | async-start | bytes 14417920 | tf_op jit(solution)/shard_map/all_gather | solution.py:12
  268.1 1.6 copy-start
  268.1 238.7 %reduce-scatter.2.cloned.1.call-start = ((), (), s32[]{:S(2)}) async-start(), calls=%async_computation.8 | async-start | bytes 3538944 | tf_op jit(solution)/shard_map/reduce_scatter | solution.py:39
Sparse Core Ops, SparseCore 0:
  127.7 102.4 all-gather.5
  263.5 75.5 all-gather.3
  341.3 76.1 all-gather.7
  432.0 74.7 reduce-scatter.1
